TPU v7x, 32 devices: a whole 2x2x4 slice. The times are simulated.
32 devices in a mesh: gr: 2 (over x), fs: 8 (over z, y), tp: 2 (over core).
Axes of the slice: x: 2, y: 2, z: 4, core: 2. Of those that a mesh axis runs over, the one named last changes fastest.
Arguments:
- prompt: bfloat16 [3072, 2048], P(('gr', 'fs', 'tp')), may hold values from -6 to 6
- norm_first: float32 [2048], P(('gr', 'fs')), may hold values from 0.1 to 1.9
- gate_first: float32 [2048, 5632], P(('gr', 'fs'), 'tp'), may hold values from -6 to 6
- up_first: float32 [2048, 5632], P(('gr', 'fs'), 'tp'), may hold values from -6 to 6
- down_first: float32 [2048, 5632], P(('gr', 'fs'), 'tp'), may hold values from -6 to 6
- norm_second: float32 [2048], P(('gr', 'fs')), may hold values from 0.1 to 1.9
- gate_second: float32 [2048, 5632], P(('gr', 'fs'), 'tp'), may hold values from -6 to 6
- up_second: float32 [2048, 5632], P(('gr', 'fs'), 'tp'), may hold values from -6 to 6
- down_second: float32 [2048, 5632], P(('gr', 'fs'), 'tp'), may hold values from -6 to 6
Outputs:
- served_gate_first: bfloat16 [2048, 5632], P(None, 'fs')
- served_up_first: bfloat16 [2048, 5632], P(None, 'fs')
- served_down_first: bfloat16 [2048, 5632], P(None, 'fs')
- served_gate_second: bfloat16 [2048, 5632], P(None, 'fs')
- served_up_second: bfloat16 [2048, 5632], P(None, 'fs')
- served_down_second: bfloat16 [2048, 5632], P(None, 'fs')
- result: bfloat16 [3072, 2048], P(('gr', 'fs', 'tp'))
All inputs are finite; a program needn't handle non-finite values.
Results may differ from a plain program's by a relative error of at most 0.015.
Values may be sent and summed in bfloat16 or wider, within the bound.
A program may use at most 128 MiB of HBM per device.

v0:
```python
import jax
import jax.numpy as jnp
from jax import lax
from jax.sharding import PartitionSpec as P

D = 2048
FF = 5632
EPS = 1e-06


def fold_rows(gain, weight):
    return (gain[:, None] * weight).astype(jnp.bfloat16)


def relayout(stacked):
    moved = lax.all_to_all(
        lax.all_to_all(stacked, "tp", split_axis=1, concat_axis=2, tiled=True),
        "fs",
        split_axis=2,
        concat_axis=1,
        tiled=True,
    )
    whole = lax.all_gather(moved, ("gr", "tp"), axis=1, tiled=True)
    matrices = stacked.shape[0]
    block_width = moved.shape[2]
    gr_size = lax.axis_size("gr")
    tp_size = lax.axis_size("tp")
    fs_size = lax.axis_size("fs")
    sub_rows = stacked.shape[1] // tp_size
    shaped = whole.reshape(matrices, gr_size, tp_size, fs_size, sub_rows, block_width)
    return shaped.transpose(0, 1, 3, 2, 4, 5).reshape(
        matrices, gr_size * fs_size * tp_size * sub_rows, block_width
    )


def half_step(residual, weights):
    gate_weight = weights[0]
    up_weight = weights[1]
    down_weight = weights[2]
    resid_f = residual.astype(jnp.float32)
    normed = (
        resid_f * lax.rsqrt(jnp.mean(resid_f * resid_f, axis=-1, keepdims=True) + EPS)
    ).astype(jnp.bfloat16)
    in_scale = D ** (-0.5)
    out_scale = FF ** (-0.5)
    tokens_in = lax.all_gather(normed, "fs", axis=0, tiled=True)
    gate_pre = jnp.dot(tokens_in, gate_weight, preferred_element_type=jnp.float32) * in_scale
    up_pre = jnp.dot(tokens_in, up_weight, preferred_element_type=jnp.float32) * in_scale
    hidden = (jax.nn.silu(gate_pre) * up_pre).astype(jnp.bfloat16)
    branch = lax.psum_scatter(
        (
            lax.dot_general(
                hidden, down_weight, (((1,), (1,)), ((), ())), preferred_element_type=jnp.float32
            )
            * out_scale
        ).astype(jnp.bfloat16),
        "fs",
        scatter_dimension=0,
        tiled=True,
    ).astype(jnp.float32)
    return (resid_f + 0.5 * branch).astype(jnp.bfloat16)


def on_device(
    prompt,
    norm_first,
    gate_first,
    up_first,
    down_first,
    norm_second,
    gate_second,
    up_second,
    down_second,
):
    first_set = jnp.stack(
        [
            fold_rows(norm_first, gate_first),
            fold_rows(norm_first, up_first),
            down_first.astype(jnp.bfloat16),
        ]
    )
    second_set = jnp.stack(
        [
            fold_rows(norm_second, gate_second),
            fold_rows(norm_second, up_second),
            down_second.astype(jnp.bfloat16),
        ]
    )
    served_first = relayout(first_set)
    middle = half_step(prompt, served_first)
    served_second = relayout(second_set)
    result = half_step(middle, served_second)
    return (
        served_first[0],
        served_first[1],
        served_first[2],
        served_second[0],
        served_second[1],
        served_second[2],
        result,
    )


def solution(mesh):
    in_specs = (
        P(("gr", "fs", "tp"), None),
        P(("gr", "fs")),
        P(("gr", "fs"), "tp"),
        P(("gr", "fs"), "tp"),
        P(("gr", "fs"), "tp"),
        P(("gr", "fs")),
        P(("gr", "fs"), "tp"),
        P(("gr", "fs"), "tp"),
        P(("gr", "fs"), "tp"),
    )
    out_specs = (
        P(None, "fs"),
        P(None, "fs"),
        P(None, "fs"),
        P(None, "fs"),
        P(None, "fs"),
        P(None, "fs"),
        P(("gr", "fs", "tp"), None),
    )
    return jax.shard_map(
        on_device, mesh=mesh, in_specs=in_specs, out_specs=out_specs, check_vma=False
    )
```

profile of v0, /device:TPU:0, one launch (start us, length us, event | category | flops | bytes accessed | tf_op | source)
XLA Modules:
  0.0 607.6 jit_solution(7273351563624397723)
XLA Ops:
  11.8 6.0 all_to_all.72
  20.5 10.8 %copy.72 = bf16[3,64,2,2816]{1,0,3,2:T(4,128)(2,1)} copy(bf16[3,64,2,2816]{3,2,1,0:T(2,128)(2,1)S(1)} %bitcast.78) | data formatting | bytes 4325376 | tf_op jit(solution)/shard_map/all_to_all | solution.py:17
  31.3 7.1 %reshape.54 = bf16[8,2,67584]{2,1,0:T(2,128)(2,1)S(1)} reshape(bf16[5632,3,64]{2,1,0:T(4,128)(2,1)} %bitcast.56) | data formatting | bytes 4325376
  38.4 57.7 %all_to_all.73 = bf16[8,2,67584]{2,1,0:T(2,128)(2,1)} all-to-all(bf16[8,2,67584]{2,1,0:T(2,128)(2,1)S(1)} %reshape.54), channel_id=1, replica_groups=mesh['gr'=2,'fs'=8,'tp'=2] {'fs'}, dimensions={0} | all-to-all | bytes 4325376 | tf_op jit(solution)/shard_map/all_to_all | solution.py:16
  96.1 8.0 %reshape.55 = bf16[5632,3,64]{2,1,0:T(4,128)(2,1)} reshape(bf16[8,2,67584]{2,1,0:T(2,128)(2,1)} %all_to_all.73) | data formatting | bytes 4325376
  104.1 9.4 %copy.55 = bf16[3,64,8,704]{3,1,2,0:T(8,128)(2,1)} copy(bf16[3,64,8,704]{1,0,3,2:T(4,128)(2,1)} %bitcast.57) | data formatting | bytes 4325376 | tf_op jit(solution)/shard_map/all_to_all | solution.py:16
  115.0 61.3 %all-gather.5.cloned.1.call-done = bf16[3,2048,704]{2,1,0:T(8,128)(2,1)} async-done(((bf16[3,512,704]{2,1,0:T(8,128)(2,1)}), bf16[3,2048,704]{2,1,0:T(8,128)(2,1)}) %all-gather.5.cloned.1.call-update) | async-done | bytes 8650768 | tf_op jit(solution)/shard_map/all_gather | solution.py:23
  184.5 54.6 %all-gather.9.cloned.1.call-done = bf16[768,2048]{1,0:T(8,128)(2,1)} async-done(((bf16[96,2048]{1,0:T(8,128)(2,1)}), bf16[768,2048]{1,0:T(8,128)(2,1)}) %all-gather.9.cloned.1.call-update) | async-done | bytes 3145744 | tf_op jit(solution)/shard_map/all_gather | solution.py:46
  239.1 5.7 fusion.16
  244.8 12.4 %multiply_convert_fusion.1 = bf16[768,2048]{1,0:T(8,128)(2,1)} fusion(bf16[2048,704]{1,0:T(8,128)(2,1)} %bitcast.64, f32[768,704]{0,1:T(8,128)} %fusion.16, bf16[768,2048]{1,0:T(8,128)(2,1)} %all-gather.9.cloned.1.call-done, bf16[2048,704]{1,0:T(8,128)(2,1)} %bitcast.62), kind=kOutput, calls=%fused_computation.1 | convolution fusion | flops 4436656128 | bytes 14221312 | tf_op jit(solution)/shard_map/dot_general | solution.py:52
  262.5 6.0 all_to_all.74
  272.5 15.1 %copy.73 = bf16[3,64,2,2816]{1,0,3,2:T(4,128)(2,1)} copy(bf16[3,64,2,2816]{3,2,1,0:T(2,128)(2,1)} %bitcast.79) | data formatting | bytes 4325376 | tf_op jit(solution)/shard_map/all_to_all | solution.py:17
  287.6 8.2 %reshape.56 = bf16[8,2,67584]{2,1,0:T(2,128)(2,1)} reshape(bf16[5632,3,64]{2,1,0:T(4,128)(2,1)} %bitcast.58) | data formatting | bytes 4325376
  295.9 67.8 %all_to_all.75 = bf16[8,2,67584]{2,1,0:T(2,128)(2,1)} all-to-all(bf16[8,2,67584]{2,1,0:T(2,128)(2,1)} %reshape.56), channel_id=1, replica_groups=mesh['gr'=2,'fs'=8,'tp'=2] {'fs'}, dimensions={0} | all-to-all | bytes 4325376 | tf_op jit(solution)/shard_map/all_to_all | solution.py:16
  363.7 8.0 %reshape.57 = bf16[5632,3,64]{2,1,0:T(4,128)(2,1)} reshape(bf16[8,2,67584]{2,1,0:T(2,128)(2,1)} %all_to_all.75) | data formatting | bytes 4325376
  371.6 9.4 %copy.62 = bf16[3,64,8,704]{3,1,2,0:T(8,128)(2,1)} copy(bf16[3,64,8,704]{1,0,3,2:T(4,128)(2,1)} %bitcast.59) | data formatting | bytes 4325376 | tf_op jit(solution)/shard_map/all_to_all | solution.py:16
  384.5 59.3 %all-gather.7.cloned.1.call-done = bf16[3,2048,704]{2,1,0:T(8,128)(2,1)} async-done(((bf16[3,512,704]{2,1,0:T(8,128)(2,1)}), bf16[3,2048,704]{2,1,0:T(8,128)(2,1)}) %all-gather.7.cloned.1.call-update) | async-done | bytes 8650768 | tf_op jit(solution)/shard_map/all_gather | solution.py:23
  453.6 52.8 %all-gather.11.cloned.1.call-done = bf16[768,2048]{1,0:T(8,128)(2,1)} async-done(((bf16[96,2048]{1,0:T(8,128)(2,1)}), bf16[768,2048]{1,0:T(8,128)(2,1)}) %all-gather.11.cloned.1.call-update) | async-done | bytes 3145744 | tf_op jit(solution)/shard_map/all_gather | solution.py:46
  506.5 6.6 %fusion.17 = f32[768,704]{0,1:T(8,128)} fusion(bf16[768,2048]{1,0:T(8,128)(2,1)} %all-gather.11.cloned.1.call-done, bf16[2048,704]{1,0:T(8,128)(2,1)} %bitcast.66), kind=kOutput, calls=%fused_computation.39 | convolution fusion | flops 2214592512 | bytes 8192000 | tf_op jit(solution)/shard_map/dot_general | solution.py:47
  513.1 12.4 %multiply_convert_fusion = bf16[768,2048]{1,0:T(8,128)(2,1)} fusion(bf16[2048,704]{1,0:T(8,128)(2,1)} %bitcast.70, f32[768,704]{0,1:T(8,128)} %fusion.17, bf16[768,2048]{1,0:T(8,128)(2,1)} %all-gather.11.cloned.1.call-done, bf16[2048,704]{1,0:T(8,128)(2,1)} %bitcast.68), kind=kOutput, calls=%fused_computation | convolution fusion | flops 4436656128 | bytes 14221312 | tf_op jit(solution)/shard_map/dot_general | solution.py:52
  525.6 4.6 copy.69
  530.1 4.6 copy.70
  541.9 4.7 copy.67
  549.3 49.1 %reduce-scatter.5.cloned.1.call-done = bf16[96,2048]{1,0:T(8,128)(2,1)} async-done(((bf16[768,2048]{1,0:T(8,128)(2,1)}), bf16[96,2048]{1,0:T(8,128)(2,1)}) %reduce-scatter.5.cloned.1.call-update) | async-done | bytes 393232 | tf_op jit(solution)/shard_map/reduce_scatter | solution.py:50
  (45 shorter events, 51.3 us)
Async XLA Ops:
  7.2 169.1 %all-gather.5.cloned.1.call-start = ((), (), s32[]{:S(2)}) async-start(), calls=%async_computation.6 | async-start | bytes 11796480 | tf_op jit(solution)/shard_map/all_gather | solution.py:23
  104.1 9.5 %copy-start.1 = (bf16[96,2048]{1,0:T(8,128)(2,1)S(1)}, bf16[96,2048]{1,0:T(8,128)(2,1)}, u32[]{:S(2)}) copy-start(bf16[96,2048]{1,0:T(8,128)(2,1)} %param.9) | copy-start | bytes 1179652
  113.5 125.6 %all-gather.9.cloned.1.call-start = ((), (), s32[]{:S(2)}) async-start(), calls=%async_computation.8 | async-start | bytes 3538944 | tf_op jit(solution)/shard_map/all_gather | solution.py:46
  114.7 266.4 %reduce-scatter.3.cloned.1.call-start = ((), (), s32[]{:S(2)}) async-start(), calls=%async_computation.9 | async-start | bytes 3538944 | tf_op jit(solution)/shard_map/reduce_scatter | solution.py:50
  257.2 0.7 copy-start.2
  257.3 186.5 %all-gather.7.cloned.1.call-start = ((), (), s32[]{:S(2)}) async-start(), calls=%async_computation.7 | async-start | bytes 11796480 | tf_op jit(solution)/shard_map/all_gather | solution.py:23
  381.0 125.4 %all-gather.11.cloned.1.call-start = ((), (), s32[]{:S(2)}) async-start(), calls=%async_computation.10 | async-start | bytes 3538944 | tf_op jit(solution)/shard_map/all_gather | solution.py:46
  384.3 214.2 %reduce-scatter.5.cloned.1.call-start = ((), (), s32[]{:S(2)}) async-start(), calls=%async_computation.11 | async-start | bytes 3538944 | tf_op jit(solution)/shard_map/reduce_scatter | solution.py:50
  541.9 4.7 copy-start
Sparse Core Ops, SparseCore 0:
  113.6 62.6 all-gather.4
  179.1 60.0 all-gather.8
  257.4 96.6 reduce-scatter.2
  381.2 62.5 all-gather.6
  446.4 60.0 all-gather.10
  525.7 72.7 reduce-scatter.4
where the time goes:
time: 615 us; the launch traced here: 608 us
  waiting for transfers between devices  277 us (45%)
  blocking collectives  138 us (22%)
  local copies, waits for them, and re-layouts  128 us (21%)
  matrix products  37.2 us (6%)
  between operations  14.4 us (2%)
  other arithmetic  11.8 us (2%)
    all_to_all x2, blocking collectives, relayout(): lax.all_to_all(lax.all_to_all(stacked, 'tp', split_axis=1, concat_axis=2,...  126 us
    all_gather x2, waiting for transfers between devices, relayout(): whole = lax.all_gather(moved, ('gr', 'tp'), axis=1, tiled=True)  121 us
    all_gather x2, waiting for transfers between devices, half_step(): tokens_in = lax.all_gather(normed, 'fs', axis=0, tiled=True)  107 us
    unnamed x16, local copies, waits for them, and re-layouts  55.2 us
    reduce_scatter x2, waiting for transfers between devices, half_step(): lax.psum_scatter((lax.dot_general(hidden, down_weight, (((1,), (1,)), (()...  49.1 us
    all_to_all x4, local copies, waits for them, and re-layouts, relayout(): lax.all_to_all(stacked, 'tp', split_axis=1, concat_axis=2, tiled=True)  32.4 us
    dot_general x2, matrix products, half_step(): lax.dot_general(hidden, down_weight, (((1,), (1,)), ((), ())), preferred_...  24.9 us
    all_to_all x2, local copies, waits for them, and re-layouts, relayout(): lax.all_to_all(lax.all_to_all(stacked, 'tp', split_axis=1, concat_axis=2,...  18.8 us
  transfers between devices with their start and end apart: 6, of which 5 were waited for; matrix products, arithmetic and copies ran while one was open for 16% of the time, Pallas kernels for 0%

commit v1 on v0

--- a/solution.py
+++ b/solution.py
@@ -14,7 +14,10 @@
 
 def relayout(stacked):
     moved = lax.all_to_all(
-        lax.all_to_all(stacked, "tp", split_axis=1, concat_axis=2, tiled=True),
+        jnp.concatenate(
+            lax.all_to_all(jnp.stack(jnp.split(stacked, lax.axis_size("tp"), axis=1)), "tp", 0, 0),
+            axis=2,
+        ),
         "fs",
         split_axis=2,
         concat_axis=1,

time: 615 us -> 589 us (0.958)
  local copies, waits for them, and re-layouts: 128 us -> 108 us
    all_to_all x6 -> x2, local copies, waits for them, and re-layouts: 51.2 us -> 18.7 us  [relayout(): lax.all_to_all(jnp.concatenate(lax.all_to_all(jnp.stack(jnp.split(stacked...]
    reshape x0 -> x2, local copies, waits for them, and re-layouts: none -> 14.8 us  [relayout(): jnp.concatenate(lax.all_to_all(jnp.stack(jnp.split(stacked, lax.axis_size...]
  transfers between devices with their start and end apart: 6 -> 6, of which waited for: 5 -> 5; matrix products, arithmetic and copies ran while one was open for 16% -> 14% of each run, Pallas kernels for 0% -> 0%
where the time goes in v1:
time: 589 us; the launch traced here: 587 us
  waiting for transfers between devices  277 us (47%)
  blocking collectives  137 us (23%)
  local copies, waits for them, and re-layouts  108 us (18%)
  matrix products  37.2 us (6%)
  between operations  14.2 us (2%)
  other arithmetic  12.2 us (2%)
    all_to_all x2, blocking collectives, relayout(): lax.all_to_all(jnp.concatenate(lax.all_to_all(jnp.stack(jnp.split(stacked...  126 us
    all_gather x2, waiting for transfers between devices, relayout(): whole = lax.all_gather(moved, ('gr', 'tp'), axis=1, tiled=True)  120 us
    all_gather x2, waiting for transfers between devices, half_step(): tokens_in = lax.all_gather(normed, 'fs', axis=0, tiled=True)  107 us
    unnamed x16, local copies, waits for them, and re-layouts  56.6 us
    reduce_scatter x2, waiting for transfers between devices, half_step(): lax.psum_scatter((lax.dot_general(hidden, down_weight, (((1,), (1,)), (()...  49.1 us
    dot_general x2, matrix products, half_step(): lax.dot_general(hidden, down_weight, (((1,), (1,)), ((), ())), preferred_...  24.9 us
    all_to_all x2, local copies, waits for them, and re-layouts, relayout(): lax.all_to_all(jnp.concatenate(lax.all_to_all(jnp.stack(jnp.split(stacked...  18.7 us
    reshape x2, local copies, waits for them, and re-layouts, relayout(): jnp.concatenate(lax.all_to_all(jnp.stack(jnp.split(stacked, lax.axis_size...  14.8 us
  transfers between devices with their start and end apart: 6, of which 5 were waited for; matrix products, arithmetic and copies ran while one was open for 14% of the time, Pallas kernels for 0%

profile of v1, /device:TPU:0, one launch (start us, length us, event | category | flops | bytes accessed | tf_op | source)
XLA Modules:
  0.0 586.6 jit_solution(13249659042891682077)
XLA Ops:
  10.3 5.5 all_to_all.46
  15.8 6.2 %copy.50 = bf16[3,64,2,2816]{1,0,3,2:T(4,128)(2,1)} copy(bf16[3,64,2,2816]{3,1,0,2:T(8,128)(2,1)S(1)} %bitcast.78) | data formatting | bytes 4325376 | tf_op jit(solution)/shard_map/reshape | solution.py:17
  22.0 7.1 %reshape.70 = bf16[8,2,67584]{2,1,0:T(2,128)(2,1)S(1)} reshape(bf16[5632,3,64]{2,1,0:T(4,128)(2,1)} %bitcast.58) | data formatting | bytes 4325376
  29.1 57.7 %all_to_all.47 = bf16[8,2,67584]{2,1,0:T(2,128)(2,1)} all-to-all(bf16[8,2,67584]{2,1,0:T(2,128)(2,1)S(1)} %reshape.70), channel_id=1, replica_groups=mesh['gr'=2,'fs'=8,'tp'=2] {'fs'}, dimensions={0} | all-to-all | bytes 4325376 | tf_op jit(solution)/shard_map/all_to_all | solution.py:16
  86.9 8.0 %reshape.71 = bf16[5632,3,64]{2,1,0:T(4,128)(2,1)} reshape(bf16[8,2,67584]{2,1,0:T(2,128)(2,1)} %all_to_all.47) | data formatting | bytes 4325376
  94.8 9.4 %copy.34 = bf16[3,64,8,704]{3,1,2,0:T(8,128)(2,1)} copy(bf16[3,64,8,704]{1,0,3,2:T(4,128)(2,1)} %bitcast.59) | data formatting | bytes 4325376 | tf_op jit(solution)/shard_map/all_to_all | solution.py:16
  106.5 60.5 %all-gather.5.cloned.1.call-done = bf16[3,2048,704]{2,1,0:T(8,128)(2,1)} async-done(((bf16[3,512,704]{2,1,0:T(8,128)(2,1)}), bf16[3,2048,704]{2,1,0:T(8,128)(2,1)}) %all-gather.5.cloned.1.call-update) | async-done | bytes 8650768 | tf_op jit(solution)/shard_map/all_gather | solution.py:26
  175.2 54.6 %all-gather.9.cloned.1.call-done = bf16[768,2048]{1,0:T(8,128)(2,1)} async-done(((bf16[96,2048]{1,0:T(8,128)(2,1)}), bf16[768,2048]{1,0:T(8,128)(2,1)}) %all-gather.9.cloned.1.call-update) | async-done | bytes 3145744 | tf_op jit(solution)/shard_map/all_gather | solution.py:49
  229.8 5.7 fusion.16
  235.5 12.4 %multiply_convert_fusion.1 = bf16[768,2048]{1,0:T(8,128)(2,1)} fusion(bf16[2048,704]{1,0:T(8,128)(2,1)} %bitcast.66, f32[768,704]{0,1:T(8,128)} %fusion.16, bf16[768,2048]{1,0:T(8,128)(2,1)} %all-gather.9.cloned.1.call-done, bf16[2048,704]{1,0:T(8,128)(2,1)} %bitcast.64), kind=kOutput, calls=%fused_computation.1 | convolution fusion | flops 4436656128 | bytes 14221312 | tf_op jit(solution)/shard_map/dot_general | solution.py:55
  251.7 6.4 %all_to_all.48 = bf16[2,3,64,2816]{3,2,1,0:T(8,128)(2,1)} all-to-all(bf16[2,3,64,2816]{3,2,1,0:T(8,128)(2,1)S(1)} %pad_maximum_fusion.3), channel_id=1, replica_groups=mesh['gr'=2,'fs'=8,'tp'=2] {'tp'}, dimensions={0} | all-to-all | bytes 4325376 | tf_op jit(solution)/shard_map/all_to_all | solution.py:18
  258.1 8.6 %copy.51 = bf16[3,64,2,2816]{1,0,3,2:T(4,128)(2,1)} copy(bf16[3,64,2,2816]{3,1,0,2:T(8,128)(2,1)} %bitcast.79) | data formatting | bytes 4325376 | tf_op jit(solution)/shard_map/reshape | solution.py:17
  266.6 8.3 %reshape.72 = bf16[8,2,67584]{2,1,0:T(2,128)(2,1)} reshape(bf16[5632,3,64]{2,1,0:T(4,128)(2,1)} %bitcast.60) | data formatting | bytes 4325376
  274.9 67.8 %all_to_all.49 = bf16[8,2,67584]{2,1,0:T(2,128)(2,1)} all-to-all(bf16[8,2,67584]{2,1,0:T(2,128)(2,1)} %reshape.72), channel_id=1, replica_groups=mesh['gr'=2,'fs'=8,'tp'=2] {'fs'}, dimensions={0} | all-to-all | bytes 4325376 | tf_op jit(solution)/shard_map/all_to_all | solution.py:16
  342.8 8.0 %reshape.73 = bf16[5632,3,64]{2,1,0:T(4,128)(2,1)} reshape(bf16[8,2,67584]{2,1,0:T(2,128)(2,1)} %all_to_all.49) | data formatting | bytes 4325376
  350.7 9.4 %copy.40 = bf16[3,64,8,704]{3,1,2,0:T(8,128)(2,1)} copy(bf16[3,64,8,704]{1,0,3,2:T(4,128)(2,1)} %bitcast.61) | data formatting | bytes 4325376 | tf_op jit(solution)/shard_map/all_to_all | solution.py:16
  363.7 59.4 %all-gather.7.cloned.1.call-done = bf16[3,2048,704]{2,1,0:T(8,128)(2,1)} async-done(((bf16[3,512,704]{2,1,0:T(8,128)(2,1)}), bf16[3,2048,704]{2,1,0:T(8,128)(2,1)}) %all-gather.7.cloned.1.call-update) | async-done | bytes 8650768 | tf_op jit(solution)/shard_map/all_gather | solution.py:26
  432.9 52.8 %all-gather.11.cloned.1.call-done = bf16[768,2048]{1,0:T(8,128)(2,1)} async-done(((bf16[96,2048]{1,0:T(8,128)(2,1)}), bf16[768,2048]{1,0:T(8,128)(2,1)}) %all-gather.11.cloned.1.call-update) | async-done | bytes 3145744 | tf_op jit(solution)/shard_map/all_gather | solution.py:49
  485.7 6.6 %fusion.17 = f32[768,704]{0,1:T(8,128)} fusion(bf16[768,2048]{1,0:T(8,128)(2,1)} %all-gather.11.cloned.1.call-done, bf16[2048,704]{1,0:T(8,128)(2,1)} %bitcast.68), kind=kOutput, calls=%fused_computation.43 | convolution fusion | flops 2214592512 | bytes 8192000 | tf_op jit(solution)/shard_map/dot_general | solution.py:50
  492.4 12.4 %multiply_convert_fusion = bf16[768,2048]{1,0:T(8,128)(2,1)} fusion(bf16[2048,704]{1,0:T(8,128)(2,1)} %bitcast.72, f32[768,704]{0,1:T(8,128)} %fusion.17, bf16[768,2048]{1,0:T(8,128)(2,1)} %all-gather.11.cloned.1.call-done, bf16[2048,704]{1,0:T(8,128)(2,1)} %bitcast.70), kind=kOutput, calls=%fused_computation | convolution fusion | flops 4436656128 | bytes 14221312 | tf_op jit(solution)/shard_map/dot_general | solution.py:55
  504.8 4.6 copy.47
  509.4 4.6 copy.48
  521.2 4.7 copy.45
  528.6 49.1 %reduce-scatter.5.cloned.1.call-done = bf16[96,2048]{1,0:T(8,128)(2,1)} async-done(((bf16[768,2048]{1,0:T(8,128)(2,1)}), bf16[96,2048]{1,0:T(8,128)(2,1)}) %reduce-scatter.5.cloned.1.call-update) | async-done | bytes 393232 | tf_op jit(solution)/shard_map/reduce_scatter | solution.py:53
  (45 shorter events, 42.6 us)
Async XLA Ops:
  7.2 159.9 %all-gather.5.cloned.1.call-start = ((), (), s32[]{:S(2)}) async-start(), calls=%async_computation.6 | async-start | bytes 11796480 | tf_op jit(solution)/shard_map/all_gather | solution.py:26
  104.2 1.0 copy-start.1
  104.2 125.6 %all-gather.9.cloned.1.call-start = ((), (), s32[]{:S(2)}) async-start(), calls=%async_computation.8 | async-start | bytes 3538944 | tf_op jit(solution)/shard_map/all_gather | solution.py:49
  106.3 253.9 %reduce-scatter.3.cloned.1.call-start = ((), (), s32[]{:S(2)}) async-start(), calls=%async_computation.9 | async-start | bytes 3538944 | tf_op jit(solution)/shard_map/reduce_scatter | solution.py:53
  247.9 0.7 copy-start.2
  248.0 175.1 %all-gather.7.cloned.1.call-start = ((), (), s32[]{:S(2)}) async-start(), calls=%async_computation.7 | async-start | bytes 11796480 | tf_op jit(solution)/shard_map/all_gather | solution.py:26
  360.1 125.6 %all-gather.11.cloned.1.call-start = ((), (), s32[]{:S(2)}) async-start(), calls=%async_computation.10 | async-start | bytes 3538944 | tf_op jit(solution)/shard_map/all_gather | solution.py:49
  363.4 214.4 %reduce-scatter.5.cloned.1.call-start = ((), (), s32[]{:S(2)}) async-start(), calls=%async_computation.11 | async-start | bytes 3538944 | tf_op jit(solution)/shard_map/reduce_scatter | solution.py:53
  521.2 4.7 copy-start
Sparse Core Ops, SparseCore 0:
  104.4 62.6 all-gather.4
  169.8 60.0 all-gather.8
  248.1 92.2 reduce-scatter.2
  360.2 62.7 all-gather.6
  425.7 60.0 all-gather.10
  504.9 72.7 reduce-scatter.4
